TPU v7x, 32 devices: a whole 2x2x4 slice. The times are simulated.
32 devices in a mesh: grp: 2 (over y), sp: 4 (over z), tp: 4 (over x, core).
Axes of the slice: x: 2, y: 2, z: 4, core: 2. Of those that a mesh axis runs over, the one named last changes fastest.
Arguments:
- residual: bfloat16 [2048, 2048], P(('grp', 'sp')), parts along dimension 0, may hold values from -6 to 6
- queries: bfloat16 [2048, 1024], P(('grp', 'sp'), 'tp'), parts along dimension 0, may hold values from -400 to 400
- keys: bfloat16 [2048, 1024], P(('grp', 'sp'), 'tp'), parts along dimension 0, may hold values from -8 to 8
- values: bfloat16 [2048, 1024], P(('grp', 'sp'), 'tp'), parts along dimension 0, may hold values from -6 to 6
- log_gates: float32 [2048, 16], P(('grp', 'sp'), 'tp'), parts along dimension 0, may hold values from -126 to 0, as said below
- w_out: bfloat16 [1024, 2048], P('tp'), may hold values from -0.75 to 0.75
- norm_gain: float32 [2048], replicated, may hold values from 0.1 to 1.9
- w_gate: bfloat16 [2048, 5632], P('sp', 'tp'), may hold values from -0.125 to 0.125
- w_up: bfloat16 [2048, 5632], P('sp', 'tp'), may hold values from -0.125 to 0.125
- w_down: bfloat16 [5632, 2048], P('tp', 'sp'), may hold values from -0.078125 to 0.078125
Outputs:
- output: bfloat16 [2048, 2048], P(('grp', 'sp', 'tp')), parts along dimension 0
There are 2 independent parts, one for each index of `grp`. A program takes and returns all parts, laid end to end along the dimension named above; an argument that names none is the same for every part. Nothing has to cross between parts.
Inputs may be any that keep to these rules, and one draw needn't show every extreme that they name: `log_gates`: never rises along positions.
All inputs are finite; a program needn't handle non-finite values.
Results may differ from a plain program's by a relative error of at most 0.014.
Values may be sent and summed in bfloat16 or wider, within the bound.
A program may use at most 128 MiB of HBM per device.

v0:
```python
import math
import jax
import jax.numpy as jnp
from jax import lax
from jax.sharding import PartitionSpec as P


def normalize(rows_in, gain):
    floats = rows_in.astype(jnp.float32)
    scaled = floats * lax.rsqrt(jnp.mean(floats * floats, axis=-1, keepdims=True) + 1e-06)
    return (scaled * gain).astype(jnp.bfloat16)


def attend(queries, keys, values, log_gates):
    row_count = queries.shape[0]
    head_count = log_gates.shape[1]
    head_width = queries.shape[1] // head_count
    score_scale = head_width ** (-0.5)
    first_row = lax.axis_index("sp") * row_count
    query_heads = queries.reshape(row_count, head_count, head_width)
    query_gates = log_gates.T
    query_positions = first_row + jnp.arange(row_count, dtype=jnp.int32)
    initial = (
        jnp.full((head_count, row_count), -1e30, jnp.float32),
        jnp.zeros((head_count, row_count), jnp.float32),
        jnp.zeros((head_count, row_count, head_width), jnp.float32),
    )
    carried = initial
    key_piece = lax.all_gather(keys.astype(jnp.float32), "sp", axis=0, tiled=True).astype(
        jnp.bfloat16
    )
    value_piece = lax.all_gather(values.astype(jnp.float32), "sp", axis=0, tiled=True).astype(
        jnp.bfloat16
    )
    gate_piece = lax.all_gather(log_gates, "sp", axis=0, tiled=True)
    length = key_piece.shape[0]
    block_rows = math.gcd(length, 2048)
    block_count = length // block_rows
    key_blocks = key_piece.reshape(block_count, block_rows, head_count, head_width)
    value_blocks = value_piece.reshape(block_count, block_rows, head_count, head_width)
    gate_blocks = gate_piece.reshape(block_count, block_rows, head_count)
    offsets = jnp.arange(block_count, dtype=jnp.int32) * block_rows

    def one_block(state, inputs):
        current_key_block, value_block, gate_block, offset = inputs

        def work(current):
            running_max, running_sum, accumulated = current
            scores = (
                jnp.einsum(
                    "qhd,khd->hqk",
                    query_heads,
                    current_key_block,
                    preferred_element_type=jnp.float32,
                )
                * score_scale
            )
            scores = scores + query_gates[:, :, None] - gate_block.T[:, None, :]
            key_positions = offset + jnp.arange(block_rows, dtype=jnp.int32)
            causal = (query_positions[:, None] >= key_positions[None, :])[None]
            scores = jnp.where(causal, scores, -1e30)
            new_max = jnp.maximum(running_max, jnp.max(scores, axis=-1))
            weights = jnp.where(causal, jnp.exp(scores - new_max[:, :, None]), 0.0)
            rescale = jnp.exp(running_max - new_max)
            running_sum = running_sum * rescale + jnp.sum(weights, axis=-1)
            product = jnp.einsum(
                "hqk,khd->hqd",
                weights.astype(jnp.bfloat16),
                value_block,
                preferred_element_type=jnp.float32,
            )
            accumulated = accumulated * rescale[:, :, None] + product
            return (new_max, running_sum, accumulated)

        state = lax.cond(offset <= first_row + row_count - 1, work, lambda current: current, state)
        return (state, None)

    carried, _ = lax.scan(one_block, carried, (key_blocks, value_blocks, gate_blocks, offsets))
    running_max, running_sum, accumulated = carried
    attended = accumulated / running_sum[:, :, None]
    return (
        attended.transpose(1, 0, 2).reshape(row_count, head_count * head_width).astype(jnp.bfloat16)
    )


def body(residual, queries, keys, values, log_gates, w_out, norm_gain, w_gate, w_up, w_down):
    attended = attend(queries, keys, values, log_gates)
    row_count = attended.shape[0]
    per_device = row_count // lax.axis_size("tp")
    my_first = lax.axis_index("tp") * per_device
    projected = lax.psum(
        jnp.dot(attended, w_out, preferred_element_type=jnp.float32).astype(jnp.bfloat16), "tp"
    ).astype(jnp.float32)
    mixed_all = (residual.astype(jnp.float32) + projected).astype(jnp.bfloat16)
    normed_all = normalize(mixed_all, norm_gain)
    mixed = lax.dynamic_slice_in_dim(mixed_all, my_first, per_device, 0)
    gate_whole = lax.all_gather(w_gate, "sp", axis=0, tiled=True)
    up_whole = lax.all_gather(w_up, "sp", axis=0, tiled=True)
    down_whole = lax.all_gather(w_down, "sp", axis=1, tiled=True)
    gate_proj = jnp.dot(normed_all, gate_whole, preferred_element_type=jnp.float32)
    up_proj = jnp.dot(normed_all, up_whole, preferred_element_type=jnp.float32)
    hidden = (jax.nn.silu(gate_proj) * up_proj).astype(jnp.bfloat16)
    down_sum = lax.psum_scatter(
        jnp.dot(hidden, down_whole, preferred_element_type=jnp.float32).astype(jnp.bfloat16),
        "tp",
        scatter_dimension=0,
        tiled=True,
    ).astype(jnp.float32)
    summed = mixed.astype(jnp.float32) + 0.5 * down_sum
    scaled = summed * lax.rsqrt(jnp.mean(summed * summed, axis=-1, keepdims=True) + 1e-06)
    return scaled.astype(jnp.bfloat16)


def solution(mesh):
    in_specs = (
        P(("grp", "sp"), None),
        P(("grp", "sp"), "tp"),
        P(("grp", "sp"), "tp"),
        P(("grp", "sp"), "tp"),
        P(("grp", "sp"), "tp"),
        P("tp", None),
        P(),
        P("sp", "tp"),
        P("sp", "tp"),
        P("tp", "sp"),
    )
    out_specs = P(("grp", "sp", "tp"), None)
    return jax.shard_map(body, mesh=mesh, in_specs=in_specs, out_specs=out_specs, check_vma=False)
```

profile of v0, /device:TPU:0, one launch (start us, length us, event | category | flops | bytes accessed | tf_op | source)
XLA Modules:
  0.0 429.7 jit_solution(2206887288210929115)
XLA Ops:
  7.4 0.0 copy-start
  7.4 0.0 all-reduce.2.cloned.1.call-start
  7.4 1.1 copy.12
  8.5 17.4 %all_gather.18 = bf16[1024,256]{0,1:T(8,128)(2,1)S(1)} all-gather(bf16[256,256]{0,1:T(8,128)(2,1)S(1)} %copy.12), channel_id=1, replica_groups=mesh['grp'=2,'sp'=4,'tp'=4] {'sp'}, dimensions={0}, use_global_device_ids=true | all-gather | bytes 655360 | tf_op jit(solution)/shard_map/all_gather | solution.py:29
  25.8 1.0 copy.13
  26.9 16.3 %all_gather.20 = bf16[1024,256]{0,1:T(8,128)(2,1)S(1)} all-gather(bf16[256,256]{0,1:T(8,128)(2,1)S(1)} %copy.13), channel_id=1, replica_groups=mesh['grp'=2,'sp'=4,'tp'=4] {'sp'}, dimensions={0}, use_global_device_ids=true | all-gather | bytes 655360 | tf_op jit(solution)/shard_map/all_gather | solution.py:32
  43.1 13.3 %all_gather.19 = f32[1024,4]{0,1:T(4,128)S(1)} all-gather(f32[256,4]{0,1:T(4,128)} %param.16), channel_id=1, replica_groups=mesh['grp'=2,'sp'=4,'tp'=4] {'sp'}, dimensions={0}, use_global_device_ids=true | all-gather | bytes 20480 | tf_op jit(solution)/shard_map/all_gather | solution.py:35
  56.5 7.0 %conditional.1 = ((f32[4,256]{1,0:T(4,128)S(1)}, f32[4,256,64]{1,2,0:T(8,128)S(1)})) conditional(s32[]{:T(128)} %convert_element_type.64, (f32[4,256]{1,0:T(4,128)S(1)}, f32[4,256,64]{1,2,0:T(8,128)S(1)}) %tuple.22, (s32[]{:T(128)}, s32[256]{0:T(256)S(1)}, bf16[256,256]{1,0:T(8,128)(2,1)}, bf16[1024,256]{0,1:T(8,128)(2,1)S(1)}, f32[4,256]{1,0:T(4,128)}, ...), branch_computations={%region_0.1_spmd, %region_1.0_spmd} | conditional | flops 288754944 | bytes 15727672 | solution.py:75
  56.5 0.0 copy-start.2
  56.6 0.2 iota_compare_fusion
  56.8 1.0 copy.14
  57.8 2.1 fusion.2
  59.9 0.0 copy-done.2
  59.9 2.0 fusion.1
  61.9 1.6 fusion.6
  63.5 0.0 copy-start.1
  63.6 0.0 copy-done
  63.6 1.4 convolution_convert_fusion
  65.0 0.0 copy-start.3
  65.0 0.0 all-reduce.2.cloned.1.call-update
  65.0 0.0 all-gather.4.cloned.1.call-start
  65.1 0.5 all-gather.4.cloned.1.call-update
  65.6 0.0 all-gather.6.cloned.1.call-start
  65.7 0.5 all-gather.6.cloned.1.call-update
  66.2 0.0 all-gather.8.cloned.1.call-start
  66.3 0.5 all-gather.8.cloned.1.call-update
  66.8 0.0 reduce-scatter.2.cloned.1.call-start
  66.8 35.4 %all-reduce.2.cloned.1.call-done = bf16[256,2048]{1,0:T(8,128)(2,1)} async-done(((bf16[256,2048]{1,0:T(8,128)(2,1)}), bf16[256,2048]{1,0:T(8,128)(2,1)}) %all-reduce.2.cloned.1.call-update) | async-done | bytes 1048592 | tf_op jit(solution)/shard_map/psum | solution.py:91
  102.2 0.0 copy-done.1
  102.2 1.7 fusion.13
  104.0 70.1 %all-gather.4.cloned.1.call-done = bf16[2048,1408]{1,0:T(8,128)(2,1)} async-done(((bf16[512,1408]{1,0:T(8,128)(2,1)}), bf16[2048,1408]{1,0:T(8,128)(2,1)}) %all-gather.4.cloned.1.call-update) | async-done | bytes 5767184 | tf_op jit(solution)/shard_map/all_gather | solution.py:97
  174.1 0.0 copy-done.3
  174.1 5.6 %fusion.18 = f32[256,1408]{1,0:T(8,128)} fusion(bf16[2048,1408]{1,0:T(8,128)(2,1)} %all-gather.4.cloned.1.call-done, bf16[256,2048]{1,0:T(8,128)(2,1)S(1)} %get-tuple-element.132, f32[2048]{0:T(1024)S(1)} %copy-done.3, f32[256]{0:T(256)S(1)} %add_rsqrt_fusion), kind=kOutput, calls=%fused_computation.29 | convolution fusion | flops 1478492160 | bytes 8266752 | tf_op jit(solution)/shard_map/dot_general | solution.py:100
  179.8 100.6 %all-gather.6.cloned.1.call-done = bf16[2048,1408]{1,0:T(8,128)(2,1)} async-done(((bf16[512,1408]{1,0:T(8,128)(2,1)}), bf16[2048,1408]{1,0:T(8,128)(2,1)}) %all-gather.6.cloned.1.call-update) | async-done | bytes 5767184 | tf_op jit(solution)/shard_map/all_gather | solution.py:98
  280.4 106.3 %all-gather.8.cloned.1.call-done = bf16[1408,2048]{1,0:T(8,128)(2,1)} async-done(((bf16[1408,512]{1,0:T(8,128)(2,1)}), bf16[1408,2048]{1,0:T(8,128)(2,1)}) %all-gather.8.cloned.1.call-update) | async-done | bytes 5767184 | tf_op jit(solution)/shard_map/all_gather | solution.py:99
  386.7 9.3 %convolution_convert_fusion.1 = bf16[256,2048]{1,0:T(8,128)(2,1)} fusion(bf16[1408,2048]{1,0:T(8,128)(2,1)} %all-gather.8.cloned.1.call-done, bf16[2048,1408]{1,0:T(8,128)(2,1)} %all-gather.6.cloned.1.call-done, f32[256,1408]{1,0:T(8,128)} %fusion.18, bf16[256,2048]{1,0:T(8,128)(2,1)S(1)} %get-tuple-element.132, f32[2048]{0:T(1024)S(1)} %copy-done.3, ...), kind=kOutput, calls=%fused_computation.21 | convolution fusion | flops 2957574144 | bytes 15082496 | tf_op jit(solution)/shard_map/dot_general | solution.py:104
  395.9 0.0 reduce-scatter.2.cloned.1.call-update
  396.0 23.2 %reduce-scatter.2.cloned.1.call-done = bf16[64,2048]{1,0:T(8,128)(2,1)} async-done(((bf16[256,2048]{1,0:T(8,128)(2,1)}), bf16[64,2048]{1,0:T(8,128)(2,1)}) %reduce-scatter.2.cloned.1.call-update) | async-done | bytes 262160 | tf_op jit(solution)/shard_map/reduce_scatter | solution.py:103
  419.2 1.2 multiply_reduce_fusion
  420.4 1.8 multiply_convert_fusion
  (9 shorter events, 0.1 us)
Async XLA Ops:
  7.4 56.2 %copy-start = (bf16[256,2048]{1,0:T(8,128)(2,1)S(1)}, bf16[256,2048]{1,0:T(8,128)(2,1)}, u32[]{:S(2)}) copy-start(bf16[256,2048]{1,0:T(8,128)(2,1)} %param.17) | copy-start | bytes 3145732
  7.4 94.9 %all-reduce.2.cloned.1.call-start = ((), (), s32[]{:S(2)}) async-start(), calls=%async_computation.1 | async-start | bytes 2097152 | tf_op jit(solution)/shard_map/psum | solution.py:91
  56.5 3.3 copy-start.2
  63.5 38.7 %copy-start.1 = (bf16[256,2048]{1,0:T(8,128)(2,1)S(1)}, bf16[256,2048]{1,0:T(8,128)(2,1)}, u32[]{:S(2)}) copy-start(bf16[256,2048]{1,0:T(8,128)(2,1)} %param.12) | copy-start | bytes 3145732
  65.0 109.1 %copy-start.3 = (f32[2048]{0:T(1024)S(1)}, f32[2048]{0:T(1024)}, u32[]{:S(2)}) copy-start(f32[2048]{0:T(1024)} %param.18) | copy-start | bytes 24580
  65.0 109.1 %all-gather.4.cloned.1.call-start = ((), (), s32[]{:S(2)}) async-start(), calls=%async_computation.2 | async-start | bytes 7208960 | tf_op jit(solution)/shard_map/all_gather | solution.py:97
  65.6 214.8 %all-gather.6.cloned.1.call-start = ((), (), s32[]{:S(2)}) async-start(), calls=%async_computation.3 | async-start | bytes 7208960 | tf_op jit(solution)/shard_map/all_gather | solution.py:98
  66.2 320.5 %all-gather.8.cloned.1.call-start = ((), (), s32[]{:S(2)}) async-start(), calls=%async_computation.4 | async-start | bytes 7208960 | tf_op jit(solution)/shard_map/all_gather | solution.py:99
  66.8 352.4 %reduce-scatter.2.cloned.1.call-start = ((), (), s32[]{:S(2)}) async-start(), calls=%async_computation.5 | async-start | bytes 1310720 | tf_op jit(solution)/shard_map/reduce_scatter | solution.py:103
Sparse Core Ops, SparseCore 0:
  65.2 37.0 all-reduce.1
  396.1 23.0 reduce-scatter.1
Sparse Core Ops, SparseCore 1:
  67.1 107.0 all-gather.3
  175.6 104.8 all-gather.5
  281.9 104.8 all-gather.7
where the time goes:
time: 430 us
  waiting for transfers between devices  337 us (78%)
  blocking collectives  47 us (11%)
  matrix products  20 us (5%)
  between operations  15.1 us (4%)
  other arithmetic  6.94 us (2%)
    all_gather x1, waiting for transfers between devices, body(): down_whole = lax.all_gather(w_down, 'sp', axis=1, tiled=True)  106 us
    all_gather x1, waiting for transfers between devices, body(): up_whole = lax.all_gather(w_up, 'sp', axis=0, tiled=True)  101 us
    all_gather x1, waiting for transfers between devices, body(): gate_whole = lax.all_gather(w_gate, 'sp', axis=0, tiled=True)  70.1 us
    psum x1, waiting for transfers between devices, body(): lax.psum(jnp.dot(attended, w_out, preferred_element_type=jnp.float32).ast...  35.4 us
    reduce_scatter x1, waiting for transfers between devices, body(): lax.psum_scatter(jnp.dot(hidden, down_whole, preferred_element_type=jnp.f...  23.2 us
    all_gather x1, blocking collectives, attend(): lax.all_gather(keys.astype(jnp.float32), 'sp', axis=0, tiled=True)  17.4 us
    all_gather x1, blocking collectives, attend(): lax.all_gather(values.astype(jnp.float32), 'sp', axis=0, tiled=True)  16.3 us
    all_gather x1, blocking collectives, attend(): gate_piece = lax.all_gather(log_gates, 'sp', axis=0, tiled=True)  13.3 us
  transfers between devices with their start and end apart: 5, of which 5 were waited for; matrix products, arithmetic and copies ran while one was open for 2% of the time, Pallas kernels for 0%

commit v1 on v0

--- a/solution.py
+++ b/solution.py
@@ -96,7 +96,12 @@
     mixed = lax.dynamic_slice_in_dim(mixed_all, my_first, per_device, 0)
     gate_whole = lax.all_gather(w_gate, "sp", axis=0, tiled=True)
     up_whole = lax.all_gather(w_up, "sp", axis=0, tiled=True)
-    down_whole = lax.all_gather(w_down, "sp", axis=1, tiled=True)
+    ring = [w_down]
+    for hop in range(3):
+        ring.append(lax.ppermute(ring[-1], "sp", [(dev, (dev + 1) % 4) for dev in range(4)]))
+    down_whole = jnp.roll(
+        jnp.concatenate(ring[::-1], axis=1), (lax.axis_index("sp") + 1) * ring[0].shape[1], axis=1
+    )
     gate_proj = jnp.dot(normed_all, gate_whole, preferred_element_type=jnp.float32)
     up_proj = jnp.dot(normed_all, up_whole, preferred_element_type=jnp.float32)
     hidden = (jax.nn.silu(gate_proj) * up_proj).astype(jnp.bfloat16)

time: 430 us -> 385 us (0.90)
  waiting for transfers between devices: 337 us -> 242 us
  starting transfers between devices: 0.17 us -> 34.2 us
  local copies, waits for them, and re-layouts: 3.14 us -> 20 us
    ppermute x0 -> x3, waiting for transfers between devices: none -> 148 us  [body(): lax.ppermute(ring[-1], 'sp', [(dev, (dev + 1) % 4) for dev in range(4)])]
    all_gather x1 -> x0, waiting for transfers between devices: 106 us -> none  [body(): down_whole = lax.all_gather(w_down, 'sp', axis=1, tiled=True)]
    all_gather x1, waiting for transfers between devices: 70.1 us -> 0.01 us  [body(): gate_whole = lax.all_gather(w_gate, 'sp', axis=0, tiled=True)]
    psum x1, waiting for transfers between devices: 35.4 us -> 0.01 us  [body(): lax.psum(jnp.dot(attended, w_out, preferred_element_type=jnp.float32).ast...]
    ppermute x0 -> x3, starting transfers between devices: none -> 34.1 us  [body(): lax.ppermute(ring[-1], 'sp', [(dev, (dev + 1) % 4) for dev in range(4)])]
    all_gather x1, waiting for transfers between devices: 101 us -> 70.6 us  [body(): up_whole = lax.all_gather(w_up, 'sp', axis=0, tiled=True)]
    unnamed x8 -> x19, local copies, waits for them, and re-layouts: 2.1 us -> 17.7 us
  transfers between devices with their start and end apart: 5 -> 7, of which waited for: 5 -> 5; matrix products, arithmetic and copies ran while one was open for 2% -> 6% of each run, Pallas kernels for 0% -> 0%
where the time goes in v1:
time: 385 us
  waiting for transfers between devices  242 us (63%)
  blocking collectives  47.1 us (12%)
  starting transfers between devices  34.2 us (9%)
  local copies, waits for them, and re-layouts  20 us (5%)
  matrix products  18.5 us (5%)
  between operations  15 us (4%)
  other arithmetic  7.37 us (2%)
    ppermute x3, waiting for transfers between devices, body(): lax.ppermute(ring[-1], 'sp', [(dev, (dev + 1) % 4) for dev in range(4)])  148 us
    all_gather x1, waiting for transfers between devices, body(): up_whole = lax.all_gather(w_up, 'sp', axis=0, tiled=True)  70.6 us
    ppermute x3, starting transfers between devices, body(): lax.ppermute(ring[-1], 'sp', [(dev, (dev + 1) % 4) for dev in range(4)])  34.1 us
    reduce_scatter x1, waiting for transfers between devices, body(): lax.psum_scatter(jnp.dot(hidden, down_whole, preferred_element_type=jnp.f...  23.1 us
    unnamed x19, local copies, waits for them, and re-layouts  17.7 us
    all_gather x1, blocking collectives, attend(): lax.all_gather(keys.astype(jnp.float32), 'sp', axis=0, tiled=True)  17.4 us
    all_gather x1, blocking collectives, attend(): lax.all_gather(values.astype(jnp.float32), 'sp', axis=0, tiled=True)  16 us
    all_gather x1, blocking collectives, attend(): gate_piece = lax.all_gather(log_gates, 'sp', axis=0, tiled=True)  13.7 us
  transfers between devices with their start and end apart: 7, of which 5 were waited for; matrix products, arithmetic and copies ran while one was open for 6% of the time, Pallas kernels for 0%

profile of v1, /device:TPU:0, one launch (start us, length us, event | category | flops | bytes accessed | tf_op | source)
XLA Modules:
  0.0 384.5 jit_solution(8581040343037315336)
XLA Ops:
  7.4 0.0 copy-start
  7.4 0.0 all-reduce.2.cloned.1.call-start
  7.4 1.1 copy.12
  8.5 17.4 %all_gather.15 = bf16[1024,256]{0,1:T(8,128)(2,1)S(1)} all-gather(bf16[256,256]{0,1:T(8,128)(2,1)S(1)} %copy.12), channel_id=1, replica_groups=mesh['grp'=2,'sp'=4,'tp'=4] {'sp'}, dimensions={0}, use_global_device_ids=true | all-gather | bytes 655360 | tf_op jit(solution)/shard_map/all_gather | solution.py:29
  25.8 13.7 %all_gather.16 = f32[1024,4]{0,1:T(4,128)S(1)} all-gather(f32[256,4]{0,1:T(4,128)} %param.16), channel_id=1, replica_groups=mesh['grp'=2,'sp'=4,'tp'=4] {'sp'}, dimensions={0}, use_global_device_ids=true | all-gather | bytes 20480 | tf_op jit(solution)/shard_map/all_gather | solution.py:35
  39.6 1.0 copy.13
  40.6 16.0 %all_gather.17 = bf16[1024,256]{0,1:T(8,128)(2,1)S(1)} all-gather(bf16[256,256]{0,1:T(8,128)(2,1)S(1)} %copy.13), channel_id=1, replica_groups=mesh['grp'=2,'sp'=4,'tp'=4] {'sp'}, dimensions={0}, use_global_device_ids=true | all-gather | bytes 655360 | tf_op jit(solution)/shard_map/all_gather | solution.py:32
  56.6 7.0 %conditional.1 = ((f32[4,256]{1,0:T(4,128)S(1)}, f32[4,256,64]{1,2,0:T(8,128)S(1)})) conditional(s32[]{:T(128)} %convert_element_type.64, (f32[4,256]{1,0:T(4,128)S(1)}, f32[4,256,64]{1,2,0:T(8,128)S(1)}) %tuple.22, (s32[]{:T(128)}, s32[256]{0:T(256)S(1)}, bf16[256,256]{1,0:T(8,128)(2,1)}, bf16[1024,256]{0,1:T(8,128)(2,1)S(1)}, f32[4,256]{1,0:T(4,128)}, ...), branch_computations={%region_0.1_spmd, %region_1.0_spmd} | conditional | flops 288754944 | bytes 15727672 | solution.py:75
  56.6 0.0 copy-start.4
  56.6 0.2 iota_compare_fusion
  56.9 1.0 copy.14
  57.9 2.0 fusion.2
  59.9 0.0 copy-done.4
  59.9 2.0 fusion.1
  62.0 1.6 fusion.6
  63.6 0.0 copy-start.1
  63.6 0.0 copy-done
  63.6 1.5 convolution_convert_fusion
  65.1 0.0 all-reduce.2.cloned.1.call-update
  65.1 0.0 all-gather.3.cloned.1.call-start
  65.2 0.5 all-gather.3.cloned.1.call-update
  65.7 0.0 all-gather.5.cloned.1.call-start
  65.8 0.5 all-gather.5.cloned.1.call-update
  66.3 0.0 reduce-scatter.2.cloned.1.call-start
  66.4 0.0 copy-done.1
  66.4 0.8 collective-permute-start
  67.1 55.6 %collective-permute-done = bf16[1408,512]{1,0:T(8,128)(2,1)S(1)} collective-permute-done((bf16[1408,512]{1,0:T(8,128)(2,1)S(1)}, bf16[1408,512]{1,0:T(8,128)(2,1)S(1)}, u32[]{:S(2)}, u32[]{:S(2)}) %collective-permute-start) | collective-permute-done | bytes 1441824 | tf_op jit(solution)/shard_map/ppermute | solution.py:101
  122.8 1.1 copy-done.2
  123.9 14.5 %collective-permute-start.1 = (bf16[1408,512]{1,0:T(8,128)(2,1)S(1)}, bf16[1408,512]{1,0:T(8,128)(2,1)}, u32[]{:S(2)}, u32[]{:S(2)}) collective-permute-start(bf16[1408,512]{1,0:T(8,128)(2,1)S(1)} %collective-permute-done), channel_id=1, source_target_pairs={{0,4},{4,8},{8,12},{12,0},{1,5},{5,9},{9,13},{13,1},{2,6},{6,10},{... | collective-permute-start | bytes 4325384 | tf_op jit(solution)/shard_map/ppermute | solution.py:101
  138.4 61.5 %collective-permute-done.1 = bf16[1408,512]{1,0:T(8,128)(2,1)} collective-permute-done((bf16[1408,512]{1,0:T(8,128)(2,1)S(1)}, bf16[1408,512]{1,0:T(8,128)(2,1)}, u32[]{:S(2)}, u32[]{:S(2)}) %collective-permute-start.1) | collective-permute-done | bytes 1441824 | tf_op jit(solution)/shard_map/ppermute | solution.py:101
  199.9 18.8 %collective-permute-start.2 = (bf16[1408,512]{1,0:T(8,128)(2,1)}, bf16[1408,512]{1,0:T(8,128)(2,1)}, u32[]{:S(2)}, u32[]{:S(2)}) collective-permute-start(bf16[1408,512]{1,0:T(8,128)(2,1)} %collective-permute-done.1), channel_id=1, source_target_pairs={{0,4},{4,8},{8,12},{12,0},{1,5},{5,9},{9,13},{13,1},{2,6},{6,10},{... | collective-permute-start | bytes 4325384 | tf_op jit(solution)/shard_map/ppermute | solution.py:101
  218.7 2.2 fusion.18
  220.9 30.4 %collective-permute-done.2 = bf16[1408,512]{1,0:T(8,128)(2,1)} collective-permute-done((bf16[1408,512]{1,0:T(8,128)(2,1)}, bf16[1408,512]{1,0:T(8,128)(2,1)}, u32[]{:S(2)}, u32[]{:S(2)}) %collective-permute-start.2) | collective-permute-done | bytes 1441824 | tf_op jit(solution)/shard_map/ppermute | solution.py:101
  251.3 2.7 constant_dynamic-update-slice_fusion.7
  253.9 2.6 constant_dynamic-update-slice_fusion.6
  256.6 1.3 constant_dynamic-update-slice_fusion.5
  257.9 1.3 constant_dynamic-update-slice_fusion.4
  259.2 2.7 constant_dynamic-update-slice_fusion.3
  261.8 2.7 constant_dynamic-update-slice_fusion.2
  264.5 1.2 constant_dynamic-update-slice_fusion.1
  265.7 1.3 constant_dynamic-update-slice_fusion
  267.0 4.5 %fusion.23 = f32[256,1408]{1,0:T(8,128)S(1)} fusion(bf16[2048,1408]{1,0:T(8,128)(2,1)} %all-gather.3.cloned.1.call-done, bf16[256,2048]{1,0:T(8,128)(2,1)S(1)} %get-tuple-element.132, f32[2048]{0:T(1024)S(1)} %copy-done.5, f32[256]{0:T(256)S(1)} %add_rsqrt_fusion), kind=kOutput, calls=%fused_computation.31 | convolution fusion | flops 1478492160 | bytes 8266752 | tf_op jit(solution)/shard_map/dot_general | solution.py:105
  271.5 70.6 %all-gather.5.cloned.1.call-done = bf16[2048,1408]{1,0:T(8,128)(2,1)} async-done(((bf16[512,1408]{1,0:T(8,128)(2,1)}), bf16[2048,1408]{1,0:T(8,128)(2,1)}) %all-gather.5.cloned.1.call-update) | async-done | bytes 5767184 | tf_op jit(solution)/shard_map/all_gather | solution.py:98
  342.1 8.9 %fusion.15 = bf16[256,2048]{1,0:T(8,128)(2,1)} fusion(bf16[1408,4096]{1,0:T(8,128)(2,1)} %constant_dynamic-update-slice_fusion, s32[]{:T(128)S(6)} %select_n.29, bf16[2048,1408]{1,0:T(8,128)(2,1)} %all-gather.5.cloned.1.call-done, f32[256,1408]{1,0:T(8,128)S(1)} %fusion.23, bf16[256,2048]{1,0:T(8,128)(2,1)S(1)} %get-tuple-element.132, ...), kind=kOutput, calls=%fused_computation.22 | convolution fusion | flops 2957574144 | bytes 15082500 | tf_op jit(solution)/shard_map/dot_general | solution.py:109
  351.0 0.0 reduce-scatter.2.cloned.1.call-update
  351.0 23.1 %reduce-scatter.2.cloned.1.call-done = bf16[64,2048]{1,0:T(8,128)(2,1)} async-done(((bf16[256,2048]{1,0:T(8,128)(2,1)}), bf16[64,2048]{1,0:T(8,128)(2,1)}) %reduce-scatter.2.cloned.1.call-update) | async-done | bytes 262160 | tf_op jit(solution)/shard_map/reduce_scatter | solution.py:108
  374.2 1.2 multiply_reduce_fusion
  375.3 1.8 multiply_convert_fusion
  (16 shorter events, 0.1 us)
Async XLA Ops:
  7.4 56.3 %copy-start = (bf16[256,2048]{1,0:T(8,128)(2,1)S(1)}, bf16[256,2048]{1,0:T(8,128)(2,1)}, u32[]{:S(2)}) copy-start(bf16[256,2048]{1,0:T(8,128)(2,1)} %param.17) | copy-start | bytes 3145732
  7.4 211.4 %all-reduce.2.cloned.1.call-start = ((), (), s32[]{:S(2)}) async-start(), calls=%async_computation.1 | async-start | bytes 2097152 | tf_op jit(solution)/shard_map/psum | solution.py:91
  56.6 3.3 copy-start.4
  63.6 2.8 copy-start.1
  65.1 201.9 %all-gather.3.cloned.1.call-start = ((), (), s32[]{:S(2)}) async-start(), calls=%async_computation.2 | async-start | bytes 7208960 | tf_op jit(solution)/shard_map/all_gather | solution.py:97
  65.7 276.4 %all-gather.5.cloned.1.call-start = ((), (), s32[]{:S(2)}) async-start(), calls=%async_computation.3 | async-start | bytes 7208960 | tf_op jit(solution)/shard_map/all_gather | solution.py:98
  66.3 307.8 %reduce-scatter.2.cloned.1.call-start = ((), (), s32[]{:S(2)}) async-start(), calls=%async_computation.4 | async-start | bytes 1310720 | tf_op jit(solution)/shard_map/reduce_scatter | solution.py:108
  66.4 56.4 %collective-permute-start = (bf16[1408,512]{1,0:T(8,128)(2,1)S(1)}, bf16[1408,512]{1,0:T(8,128)(2,1)S(1)}, u32[]{:S(2)}, u32[]{:S(2)}) collective-permute-start(bf16[1408,512]{1,0:T(8,128)(2,1)S(1)} %copy-done.1), channel_id=1, source_target_pairs={{0,4},{4,8},{8,12},{12,0},{1,5},{5,9},{9,13},{13,1},{2,6},{6,10},{... | collective-permute-start | bytes 4325384 | tf_op jit(solution)/shard_map/ppermute | solution.py:101
  122.8 1.1 copy-start.2
  123.9 76.0 %collective-permute-start.1 = (bf16[1408,512]{1,0:T(8,128)(2,1)S(1)}, bf16[1408,512]{1,0:T(8,128)(2,1)}, u32[]{:S(2)}, u32[]{:S(2)}) collective-permute-start(bf16[1408,512]{1,0:T(8,128)(2,1)S(1)} %collective-permute-done), channel_id=1, source_target_pairs={{0,4},{4,8},{8,12},{12,0},{1,5},{5,9},{9,13},{13,1},{2,6},{6,10},{... | collective-permute-start | bytes 4325384 | tf_op jit(solution)/shard_map/ppermute | solution.py:101
  199.9 51.4 %collective-permute-start.2 = (bf16[1408,512]{1,0:T(8,128)(2,1)}, bf16[1408,512]{1,0:T(8,128)(2,1)}, u32[]{:S(2)}, u32[]{:S(2)}) collective-permute-start(bf16[1408,512]{1,0:T(8,128)(2,1)} %collective-permute-done.1), channel_id=1, source_target_pairs={{0,4},{4,8},{8,12},{12,0},{1,5},{5,9},{9,13},{13,1},{2,6},{6,10},{... | collective-permute-start | bytes 4325384 | tf_op jit(solution)/shard_map/ppermute | solution.py:101
  218.7 37.8 %copy-start.3 = (bf16[1408,512]{1,0:T(8,128)(2,1)S(1)}, bf16[1408,512]{1,0:T(8,128)(2,1)}, u32[]{:S(2)}) copy-start(bf16[1408,512]{1,0:T(8,128)(2,1)} %copy-done.2) | copy-start | bytes 4325380
  261.8 5.2 %copy-start.5 = (f32[2048]{0:T(1024)S(1)}, f32[2048]{0:T(1024)}, u32[]{:S(2)}) copy-start(f32[2048]{0:T(1024)} %param.18) | copy-start | bytes 24580
Sparse Core Ops, SparseCore 0:
  65.3 36.8 all-reduce.1
  351.1 22.9 reduce-scatter.1
Sparse Core Ops, SparseCore 1:
  67.2 165.1 all-gather.2
  233.8 108.3 all-gather.4
